TPU v7x, 32 devices: a whole 2x2x4 slice. The times are simulated.
32 devices in a mesh: ep: 16 (over z, x, core), tp: 2 (over y).
Axes of the slice: x: 2, y: 2, z: 4, core: 2. Of those that a mesh axis runs over, the one named last changes fastest.
Arguments:
- residual_in: bfloat16 [240, 1536], P('ep'), may hold values from -6 to 6
- rec_state: bfloat16 [240, 12, 128, 128], P('ep', 'tp'), may hold values from -6 to 6
- mix_gain: float32 [1536], replicated, may hold values from 0.1 to 1.9
- w_query: bfloat16 [1536, 1536], P('tp', 'ep'), may hold values from -0.15625 to 0.15625
- w_forget: bfloat16 [1536, 1536], P('tp', 'ep'), may hold values from -0.15625 to 0.15625
- w_input: bfloat16 [1536, 1536], P('tp', 'ep'), may hold values from -0.15625 to 0.15625
- w_gate: bfloat16 [1536, 1536], P('tp', 'ep'), may hold values from -0.15625 to 0.15625
- lower_bound: float32 [1536], P('tp'), may hold values from 0 to 0.9
- head_gain: float32 [128], replicated, may hold values from 0.1 to 1.9
- w_out: bfloat16 [1536, 1536], P('tp', 'ep'), may hold values from -0.15625 to 0.15625
- ffn_gain: float32 [1536], replicated, may hold values from 0.1 to 1.9
- route_ids: int32 [240, 6], P('ep'), may hold values from 0 to 15, all different within a row; in each aligned block of 15 rows (0 to 14, 15 to 29, ...) at most 6 rows name the same one
- route_weight: float32 [240, 6], P('ep'), may hold values from 0.2 to 1
- expert_gate: bfloat16 [16, 1536, 512], P('ep', None, 'tp'), may hold values from -0.15625 to 0.15625
- expert_up: bfloat16 [16, 1536, 512], P('ep', None, 'tp'), may hold values from -0.15625 to 0.15625
- expert_down: bfloat16 [16, 512, 1536], P('ep', 'tp'), may hold values from -0.25 to 0.25
Outputs:
- layer_out: bfloat16 [240, 1536], P('ep', 'tp')
- new_state: bfloat16 [240, 12, 128, 128], P('ep', 'tp')
Inputs may be any that keep to these rules, and one draw needn't show every extreme that they name: `route_ids`: each row names 6 different experts. Among the rows of one device no expert is named more than 6 times, and in every draw some device names some expert exactly 6 times.
All inputs are finite; a program needn't handle non-finite values.
Results may differ from a plain program's by a relative error of at most 0.016.
Values may be sent and summed in bfloat16 or wider, within the bound.
No kernel may reach another device: no remote copies, remote signals or barrier semaphores. Data moves between devices by JAX's collectives and lax.ppermute only.
A program may use at most 64 MiB of HBM per device.

v0:
```python
import jax
import jax.numpy as jnp
from jax import lax
from jax.sharding import PartitionSpec as P

rms_eps = 1e-06


def rms_scale(values, gain):
    return values * lax.rsqrt(jnp.mean(values * values, axis=-1, keepdims=True) + rms_eps) * gain


def rounded(values):
    return lax.optimization_barrier(values.astype(jnp.bfloat16)).astype(jnp.float32)


def recurrence(lower_bound, head_gain, state_block, query_raw, forget_raw, input_raw, gate_raw):
    seq_count = state_block.shape[0]
    heads_local = state_block.shape[1]
    head_size = state_block.shape[2]
    head_shape = (seq_count, heads_local, head_size)
    forget = lower_bound + (1.0 - lower_bound) * jax.nn.sigmoid(forget_raw)
    query_act = jax.nn.silu(query_raw).reshape(head_shape)
    key_act = (1.0 - forget).reshape(head_shape)
    forget_heads = forget.reshape(head_shape)
    value_act = input_raw.reshape(head_shape)
    state_next = (
        forget_heads[:, :, :, None] * state_block.astype(jnp.float32)
        + key_act[:, :, :, None] * value_act[:, :, None, :]
    )
    readout = jnp.einsum("shk,shkv->shv", query_act, state_next, precision=lax.Precision.HIGHEST)
    gate_heads = jax.nn.silu(gate_raw).reshape(head_shape)
    heads_out = rms_scale(readout, head_gain) * gate_heads
    return (
        state_next.astype(jnp.bfloat16),
        heads_out.reshape(seq_count, heads_local * head_size).astype(jnp.bfloat16),
    )


def shards(
    residual_in,
    rec_state,
    mix_gain,
    w_query,
    w_forget,
    w_input,
    w_gate,
    lower_bound,
    head_gain,
    w_out,
    ffn_gain,
    route_ids,
    route_weight,
    expert_gate,
    expert_up,
    expert_down,
):
    tp_count = lax.axis_size("tp")
    tp_rank = lax.axis_index("tp")
    ep_count = lax.axis_size("ep")
    seq_count = residual_in.shape[0]
    model_width = residual_in.shape[1]
    quarter = model_width // tp_count
    residual = residual_in.astype(jnp.float32)
    normed = rms_scale(residual, mix_gain).astype(jnp.bfloat16)
    own_rows = lax.dynamic_slice_in_dim(normed, tp_rank * quarter, quarter, 1)
    rows_piece = lax.all_gather(own_rows, "ep", axis=0, tiled=True)
    partial_proj = jnp.stack(
        [
            jnp.dot(rows_piece, weight, preferred_element_type=jnp.float32)
            for weight in (w_query, w_forget, w_input, w_gate)
        ],
        axis=1,
    )
    arrived = lax.all_to_all(partial_proj, "ep", split_axis=0, concat_axis=2, tiled=True)
    summed = lax.psum_scatter(arrived, "tp", scatter_dimension=2, tiled=True)
    projected = rounded(summed)
    new_state, heads_out = recurrence(
        lower_bound,
        head_gain,
        rec_state,
        projected[:, 0],
        projected[:, 1],
        projected[:, 2],
        projected[:, 3],
    )
    partial_mix = jnp.dot(
        lax.all_gather(heads_out, "ep", axis=0, tiled=True),
        w_out,
        preferred_element_type=jnp.float32,
    )
    mixed_home = lax.all_to_all(
        partial_mix.astype(jnp.bfloat16), "ep", split_axis=0, concat_axis=1, tiled=True
    ).astype(partial_mix.dtype)
    mixed = lax.psum(mixed_home.astype(jnp.bfloat16), "tp").astype(jnp.float32)
    after_mix = rounded(residual + mixed)
    normed_ffn = rms_scale(after_mix, ffn_gain).astype(jnp.bfloat16)
    exp_dev = expert_gate.shape[0]
    experts_all = ep_count * exp_dev
    top_count = route_ids.shape[1]
    capacity = max(2, seq_count * top_count // experts_all + 1)
    flat_ids = route_ids.reshape(-1)
    onehot = (flat_ids[:, None] == jnp.arange(experts_all, dtype=jnp.int32)[None, :]).astype(
        jnp.int32
    )
    slot_rank = jnp.sum(jnp.cumsum(onehot, axis=0) * onehot, axis=1) - 1
    slot_index = flat_ids * capacity + slot_rank
    placer_int = (
        jnp.arange(experts_all * capacity, dtype=jnp.int32)[:, None] == slot_index[None, :]
    ).astype(jnp.int32)
    placer = jnp.sum(
        placer_int.reshape(experts_all * capacity, seq_count, top_count), axis=2
    ).astype(jnp.bfloat16)
    buffer = (
        jnp.dot(placer, normed_ffn, preferred_element_type=jnp.float32)
        .astype(jnp.bfloat16)
        .reshape(experts_all, capacity, model_width)
    )
    received = lax.all_to_all(buffer, "ep", split_axis=0, concat_axis=0, tiled=True)
    slot_count = received.shape[1]
    grouped = received.reshape(ep_count, exp_dev, slot_count, model_width)
    gate_part = jnp.einsum(
        "sjnd,jdf->sjnf", grouped, expert_gate, preferred_element_type=jnp.float32
    )
    up_part = jnp.einsum("sjnd,jdf->sjnf", grouped, expert_up, preferred_element_type=jnp.float32)
    hidden = (jax.nn.silu(gate_part) * up_part).astype(jnp.bfloat16)
    down_part = jnp.einsum(
        "sjnf,jfd->sjnd", hidden, expert_down, preferred_element_type=jnp.float32
    )
    summed_down = lax.psum_scatter(
        down_part.astype(jnp.bfloat16), "tp", scatter_dimension=3, tiled=True
    )
    returned = summed_down.reshape(experts_all, slot_count, quarter)
    gathered_back = lax.all_to_all(returned, "ep", split_axis=0, concat_axis=0, tiled=True)
    flat_back = gathered_back.reshape(experts_all * capacity, quarter)
    picked = (
        jnp.take(flat_back, slot_index, axis=0)
        .astype(jnp.float32)
        .reshape(seq_count, top_count, quarter)
    )
    expert_sum = jnp.sum(route_weight[:, :, None] * picked, axis=1)
    own_mix = lax.dynamic_slice_in_dim(after_mix, tp_rank * quarter, quarter, 1)
    layer_out = (own_mix + expert_sum).astype(jnp.bfloat16)
    return (layer_out, new_state)


def solution(mesh):
    in_specs = (
        P("ep", None),
        P("ep", "tp", None, None),
        P(),
        P("tp", "ep"),
        P("tp", "ep"),
        P("tp", "ep"),
        P("tp", "ep"),
        P("tp"),
        P(),
        P("tp", "ep"),
        P(),
        P("ep", None),
        P("ep", None),
        P("ep", None, "tp"),
        P("ep", None, "tp"),
        P("ep", "tp", None),
    )
    out_specs = (P("ep", "tp"), P("ep", "tp", None, None))
    return jax.shard_map(shards, mesh=mesh, in_specs=in_specs, out_specs=out_specs, check_vma=False)
```

profile of v0, /device:TPU:0, one launch (start us, length us, event | category | flops | bytes accessed | tf_op | source)
XLA Modules:
  0.0 206.5 jit_solution(8427857682327721564)
XLA Ops:
  9.9 24.1 %all-gather = bf16[16,15,768]{2,1,0:T(8,128)(2,1)S(1)} all-gather(bf16[1,15,768]{2,1,0:T(8,128)(2,1)S(1)} %fusion.36), channel_id=1, replica_groups=mesh['ep'=16,'tp'=2] {'ep'}, dimensions={0}, use_global_device_ids=true | all-gather | bytes 391680 | tf_op jit(solution)/shard_map/all_gather | solution.py:67
  34.1 1.2 convolution_bitcast_fusion.2
  35.3 1.2 convolution_bitcast_fusion.3
  37.7 1.2 convolution_bitcast_fusion.5
  39.9 3.6 %all-to-all-start = ((f32[240,4,96]{2,1,0:T(4,128)}), f32[240,4,96]{2,1,0:T(4,128)S(1)}, u32[]{:S(2)}, u32[]{:S(2)}) async-start(f32[240,4,96]{2,1,0:T(4,128)} %copy.50), calls=%async_computation | async-start | bytes 983040 | tf_op jit(solution)/shard_map/all_to_all | solution.py:75
  43.9 13.2 %all-to-all-done = f32[240,4,96]{2,1,0:T(4,128)S(1)} async-done(((f32[240,4,96]{2,1,0:T(4,128)}), f32[240,4,96]{2,1,0:T(4,128)S(1)}, u32[]{:S(2)}, u32[]{:S(2)}) %all-to-all-start) | async-done | bytes 368672 | tf_op jit(solution)/shard_map/all_to_all | solution.py:75
  57.2 7.4 %copy.65 = f32[15,4,16,96]{1,0,3,2:T(8,128)} copy(f32[15,4,16,96]{3,1,0,2:T(4,128)S(1)} %bitcast.97) | data formatting | bytes 737280
  64.5 9.6 %reshape.217 = f32[1536,60]{1,0:T(8,128)} reshape(f32[1536,15,4]{2,1,0:T(8,128)} %bitcast.95) | data formatting | bytes 737280
  74.6 16.6 %reduce-scatter.7.cloned.1.call-done = f32[768,60]{1,0:T(8,128)} async-done(((f32[1536,60]{1,0:T(8,128)}), f32[768,60]{1,0:T(8,128)}) %reduce-scatter.7.cloned.1.call-update) | async-done | bytes 184336
  91.1 5.3 %reshape.218 = bf16[768,15,4]{2,1,0:T(8,128)(2,1)} reshape(f32[768,60]{1,0:T(8,128)} %reduce-scatter.7.cloned.1.call-done) | data formatting | bytes 276480
  96.4 4.4 %copy.64 = bf16[15,4,768]{2,1,0:T(4,128)(2,1)S(1)} copy(bf16[15,4,768]{1,0,2:T(8,128)(2,1)} %bitcast.96) | data formatting | bytes 184320
  101.6 8.9 %fusion.1 = f32[15,6,1,128]{3,2,1,0:T(1,128)S(1)} fusion(bf16[15,6,128,128]{3,2,1,0:T(8,128)(2,1)} %param.17, f32[15,6,128]{2,1,0:T(8,128)S(1)} %mul.167, f32[15,6,128]{2,1,0:T(8,128)S(1)} %get-tuple-element.8, f32[15,6,128]{2,1,0:T(8,128)S(1)} %get-tuple-element.9, f32[15,6,128,1]{2,1,0,3:T(8,128)S(1)} %multiply_bitcast_fusion), kind=kOutput, calls=%fused_computation.3 | convolution fusion | flops 23592960 | bytes 3179520 | tf_op jit(solution)/shard_map/shk,shkv->shv/dot_general | solution.py:31
  110.8 22.4 %all-gather.1 = bf16[16,15,768]{2,1,0:T(8,128)(2,1)S(1)} all-gather(bf16[1,15,768]{2,1,0:T(8,128)(2,1)S(1)} %reshape.209), channel_id=1, replica_groups=mesh['ep'=16,'tp'=2] {'ep'}, dimensions={0}, use_global_device_ids=true | all-gather | bytes 391680 | tf_op jit(solution)/shard_map/all_gather | solution.py:88
  133.3 1.2 convolution_convert_fusion.2
  135.3 3.5 %all-to-all-start.1 = ((bf16[16,15,96]{2,1,0:T(8,128)(2,1)}), bf16[16,15,96]{2,1,0:T(8,128)(2,1)S(1)}, u32[]{:S(2)}, u32[]{:S(2)}) async-start(bf16[16,15,96]{2,1,0:T(8,128)(2,1)} %all_to_all.37), calls=%async_computation.1 | async-start | bytes 131072 | tf_op jit(solution)/shard_map/all_to_all | solution.py:92
  138.9 6.7 %all-to-all-done.1 = bf16[16,15,96]{2,1,0:T(8,128)(2,1)S(1)} async-done(((bf16[16,15,96]{2,1,0:T(8,128)(2,1)}), bf16[16,15,96]{2,1,0:T(8,128)(2,1)S(1)}, u32[]{:S(2)}, u32[]{:S(2)}) %all-to-all-start.1) | async-done | bytes 46112 | tf_op jit(solution)/shard_map/all_to_all | solution.py:92
  145.8 7.7 %psum.7 = bf16[15,1536]{1,0:T(8,128)(2,1)S(1)} all-reduce(bf16[15,1536]{1,0:T(8,128)(2,1)S(1)} %all_to_all.40), channel_id=1, replica_groups=mesh['ep'=16,'tp'=2] {'tp'}, use_global_device_ids=true, to_apply=%region_3.4 | all-reduce | flops 23040 | bytes 92160 | tf_op jit(solution)/shard_map/psum | solution.py:95
  154.0 14.8 %all_to_all.47 = bf16[16,6,1536]{2,1,0:T(8,128)(2,1)S(1)} all-to-all(bf16[16,6,1536]{2,1,0:T(8,128)(2,1)S(1)} %reshape.192), channel_id=1, replica_groups=mesh['ep'=16,'tp'=2] {'ep'}, dimensions={0} | all-to-all | bytes 589824 | tf_op jit(solution)/shard_map/all_to_all | solution.py:119
  169.1 1.4 fusion.5
  170.7 11.0 %reduce-scatter.5.cloned.1.call-done = bf16[16,1,6,768]{3,0,2,1:T(8,128)(2,1)} async-done(((bf16[16,1,6,1536]{3,0,2,1:T(8,128)(2,1)}), bf16[16,1,6,768]{3,0,2,1:T(8,128)(2,1)}) %reduce-scatter.5.cloned.1.call-update) | async-done | bytes 147472 | tf_op jit(solution)/shard_map/reduce_scatter | solution.py:130
  181.7 1.6 copy.60
  183.3 5.6 %all-to-all-start.3 = ((bf16[16,6,768]{2,1,0:T(8,128)(2,1)}), bf16[16,6,768]{2,1,0:T(8,128)(2,1)S(1)}, u32[]{:S(2)}, u32[]{:S(2)}) async-start(bf16[16,6,768]{2,1,0:T(8,128)(2,1)} %copy.60), calls=%async_computation.4 | async-start | bytes 393216 | tf_op jit(solution)/shard_map/all_to_all | solution.py:134
  188.9 6.7 %fusion = bf16[15,6,128,128]{3,2,1,0:T(8,128)(2,1)} fusion(bf16[15,6,128,128]{3,2,1,0:T(8,128)(2,1)} %param.17, f32[15,6,128]{2,1,0:T(8,128)S(1)} %mul.167, f32[15,6,128]{2,1,0:T(8,128)S(1)} %get-tuple-element.8, f32[15,6,128]{2,1,0:T(8,128)S(1)} %get-tuple-element.9), kind=kLoop, calls=%fused_computation.2 | loop fusion | flops 7372800 | bytes 6036480 | tf_op jit(solution)/shard_map/convert_element_type | solution.py:35
  195.6 2.3 %all-to-all-done.3 = bf16[16,6,768]{2,1,0:T(8,128)(2,1)S(1)} async-done(((bf16[16,6,768]{2,1,0:T(8,128)(2,1)}), bf16[16,6,768]{2,1,0:T(8,128)(2,1)S(1)}, u32[]{:S(2)}, u32[]{:S(2)}) %all-to-all-start.3) | async-done | bytes 147488 | tf_op jit(solution)/shard_map/all_to_all | solution.py:134
  (76 shorter events, 10.6 us)
Async XLA Ops:
  7.2 161.9 %copy-start = (bf16[1,256,1536]{2,1,0:T(8,128)(2,1)S(1)}, bf16[1,256,1536]{2,1,0:T(8,128)(2,1)}, u32[]{:S(2)}) copy-start(bf16[1,256,1536]{2,1,0:T(8,128)(2,1)} %param.31) | copy-start | bytes 2359300
  7.2 36.3 %copy-start.6 = (s32[15,6]{0,1:T(8,128)S(1)}, s32[15,6]{0,1:T(8,128)}, u32[]{:S(2)}) copy-start(s32[15,6]{0,1:T(8,128)} %param.27) | copy-start | bytes 1084
  39.9 17.3 %all-to-all-start = ((f32[240,4,96]{2,1,0:T(4,128)}), f32[240,4,96]{2,1,0:T(4,128)S(1)}, u32[]{:S(2)}, u32[]{:S(2)}) async-start(f32[240,4,96]{2,1,0:T(4,128)} %copy.50), calls=%async_computation | async-start | bytes 983040 | tf_op jit(solution)/shard_map/all_to_all | solution.py:75
  43.4 47.7 %reduce-scatter.7.cloned.1.call-start = ((), (), s32[]{:S(2)}) async-start(), calls=%async_computation.7 | async-start | bytes 1179648
  64.5 10.0 %copy-start.4 = (f32[768]{0:T(1024)S(1)}, f32[768]{0:T(1024)}, u32[]{:S(2)}) copy-start(f32[768]{0:T(1024)} %param.23) | copy-start | bytes 9220
  96.4 14.2 %copy-start.8 = (f32[128]{0:T(128)S(1)}, f32[128]{0:T(128)}, u32[]{:S(2)}) copy-start(f32[128]{0:T(128)} %param.24) | copy-start | bytes 1540
  100.8 52.7 %copy-start.3 = (bf16[15,1536]{1,0:T(8,128)(2,1)S(1)}, bf16[15,1536]{1,0:T(8,128)(2,1)}, u32[]{:S(2)}) copy-start(bf16[15,1536]{1,0:T(8,128)(2,1)} %param.16) | copy-start | bytes 138244
  100.8 52.8 %copy-start.5 = (f32[1536]{0:T(1024)S(1)}, f32[1536]{0:T(1024)}, u32[]{:S(2)}) copy-start(f32[1536]{0:T(1024)} %param.26) | copy-start | bytes 18436
  101.4 67.4 %copy-start.1 = (bf16[1,1536,256]{2,1,0:T(8,128)(2,1)S(1)}, bf16[1,1536,256]{2,1,0:T(8,128)(2,1)}, u32[]{:S(2)}) copy-start(bf16[1,1536,256]{2,1,0:T(8,128)(2,1)} %param.29) | copy-start | bytes 2359300
  101.5 67.6 %copy-start.2 = (bf16[1,1536,256]{2,1,0:T(8,128)(2,1)S(1)}, bf16[1,1536,256]{2,1,0:T(8,128)(2,1)}, u32[]{:S(2)}) copy-start(bf16[1,1536,256]{2,1,0:T(8,128)(2,1)} %param.30) | copy-start | bytes 2359300
  101.5 69.0 %copy-start.7 = (f32[15,6]{0,1:T(8,128)S(1)}, f32[15,6]{0,1:T(8,128)}, u32[]{:S(2)}) copy-start(f32[15,6]{0,1:T(8,128)} %param.28) | copy-start | bytes 1084
  135.3 10.4 %all-to-all-start.1 = ((bf16[16,15,96]{2,1,0:T(8,128)(2,1)}), bf16[16,15,96]{2,1,0:T(8,128)(2,1)S(1)}, u32[]{:S(2)}, u32[]{:S(2)}) async-start(bf16[16,15,96]{2,1,0:T(8,128)(2,1)} %all_to_all.37), calls=%async_computation.1 | async-start | bytes 131072 | tf_op jit(solution)/shard_map/all_to_all | solution.py:92
  138.8 42.9 %reduce-scatter.5.cloned.1.call-start = ((), (), s32[]{:S(2)}) async-start(), calls=%async_computation.6 | async-start | bytes 442368 | tf_op jit(solution)/shard_map/reduce_scatter | solution.py:130
  183.3 14.6 %all-to-all-start.3 = ((bf16[16,6,768]{2,1,0:T(8,128)(2,1)}), bf16[16,6,768]{2,1,0:T(8,128)(2,1)S(1)}, u32[]{:S(2)}, u32[]{:S(2)}) async-start(bf16[16,6,768]{2,1,0:T(8,128)(2,1)} %copy.60), calls=%async_computation.4 | async-start | bytes 393216 | tf_op jit(solution)/shard_map/all_to_all | solution.py:134
Sparse Core Ops, SparseCore 0:
  74.3 16.7 reduce-scatter.6
  170.6 11.0 reduce-scatter.4
where the time goes:
time: 207 us; the launch traced here: 206 us
  blocking collectives  69 us (33%)
  waiting for transfers between devices  49.8 us (24%)
  local copies, waits for them, and re-layouts  32.9 us (16%)
  matrix products  16.7 us (8%)
  between operations  14.4 us (7%)
  starting transfers between devices  12.8 us (6%)
  other arithmetic  10.9 us (5%)
    unnamed x27, local copies, waits for them, and re-layouts  27.2 us
    all_gather x1, blocking collectives, shards(): rows_piece = lax.all_gather(own_rows, 'ep', axis=0, tiled=True)  24.1 us
    all_gather x1, blocking collectives, shards(): lax.all_gather(heads_out, 'ep', axis=0, tiled=True)  22.4 us
    unnamed x3, waiting for transfers between devices  16.6 us
    all_to_all x1, blocking collectives, shards(): lax.all_to_all(buffer, 'ep', split_axis=0, concat_axis=0, tiled=True)  14.8 us
    all_to_all x1, waiting for transfers between devices, shards(): lax.all_to_all(partial_proj, 'ep', split_axis=0, concat_axis=2, tiled=True)  13.2 us
    reduce_scatter x1, waiting for transfers between devices, shards(): lax.psum_scatter(down_part.astype(jnp.bfloat16), 'tp', scatter_dimension=...  11 us
    dot_general x1, matrix products, recurrence(): jnp.einsum('shk,shkv->shv', query_act, state_next, precision=lax.Precisio...  8.93 us
  transfers between devices with their start and end apart: 5, of which 5 were waited for; matrix products, arithmetic and copies ran while one was open for 4% of the time, Pallas kernels for 0%

commit v1 on v0

--- a/solution.py
+++ b/solution.py
@@ -72,7 +72,9 @@
         ],
         axis=1,
     )
-    arrived = lax.all_to_all(partial_proj, "ep", split_axis=0, concat_axis=2, tiled=True)
+    arrived = jnp.concatenate(
+        lax.all_to_all(jnp.stack(jnp.split(partial_proj, lax.axis_size("ep"), 0)), "ep", 0, 0), 2
+    )
     summed = lax.psum_scatter(arrived, "tp", scatter_dimension=2, tiled=True)
     projected = rounded(summed)
     new_state, heads_out = recurrence(

time: 207 us -> 221 us (1.068)
  local copies, waits for them, and re-layouts: 32.9 us -> 47.6 us
    unnamed x27 -> x54, local copies, waits for them, and re-layouts: 27.2 us -> 39 us
    another operation x1 -> x2, local copies, waits for them, and re-layouts: 0.98 us -> 3.91 us  [shards(): jnp.stack(jnp.split(partial_proj, lax.axis_size('ep'), 0))]
where the time goes in v1:
time: 221 us; the launch traced here: 220 us
  blocking collectives  69.1 us (31%)
  waiting for transfers between devices  49.1 us (22%)
  local copies, waits for them, and re-layouts  47.6 us (22%)
  matrix products  15.5 us (7%)
  between operations  14.5 us (7%)
  starting transfers between devices  12.9 us (6%)
  other arithmetic  11.5 us (5%)
    unnamed x54, local copies, waits for them, and re-layouts  39 us
    all_gather x1, blocking collectives, shards(): rows_piece = lax.all_gather(own_rows, 'ep', axis=0, tiled=True)  24.1 us
    all_gather x1, blocking collectives, shards(): lax.all_gather(heads_out, 'ep', axis=0, tiled=True)  22.5 us
    unnamed x3, waiting for transfers between devices  16 us
    all_to_all x1, blocking collectives, shards(): lax.all_to_all(buffer, 'ep', split_axis=0, concat_axis=0, tiled=True)  14.8 us
    all_to_all x1, waiting for transfers between devices, shards(): lax.all_to_all(jnp.stack(jnp.split(partial_proj, lax.axis_size('ep'), 0))...  13.2 us
    reduce_scatter x1, waiting for transfers between devices, shards(): lax.psum_scatter(down_part.astype(jnp.bfloat16), 'tp', scatter_dimension=...  10.9 us
    dot_general x1, matrix products, recurrence(): jnp.einsum('shk,shkv->shv', query_act, state_next, precision=lax.Precisio...  8.88 us
  transfers between devices with their start and end apart: 5, of which 5 were waited for; matrix products, arithmetic and copies ran while one was open for 4% of the time, Pallas kernels for 0%

profile of v1, /device:TPU:0, one launch (start us, length us, event | category | flops | bytes accessed | tf_op | source)
XLA Modules:
  0.0 220.3 jit_solution(10295439069672509291)
XLA Ops:
  9.9 24.1 %all-gather = bf16[16,15,768]{2,1,0:T(8,128)(2,1)S(1)} all-gather(bf16[1,15,768]{2,1,0:T(8,128)(2,1)S(1)} %fusion.52), channel_id=1, replica_groups=mesh['ep'=16,'tp'=2] {'ep'}, dimensions={0}, use_global_device_ids=true | all-gather | bytes 391680 | tf_op jit(solution)/shard_map/all_gather | solution.py:67
  34.2 1.2 convolution_bitcast_fusion.2
  35.3 1.2 convolution_bitcast_fusion.3
  36.5 1.2 convolution_bitcast_fusion.4
  50.6 3.1 %copy.64 = f32[16,15,4,96]{3,2,1,0:T(4,128)} copy(f32[16,15,4,96]{1,3,2,0:T(8,128)} %fusion.17) | data formatting | bytes 737280 | tf_op jit(solution)/shard_map/stack | solution.py:76
  53.7 3.6 %all-to-all-start = ((f32[16,15,4,96]{3,2,1,0:T(4,128)}), f32[16,15,4,96]{3,2,1,0:T(4,128)S(1)}, u32[]{:S(2)}, u32[]{:S(2)}) async-start(f32[16,15,4,96]{3,2,1,0:T(4,128)} %copy.64), calls=%async_computation | async-start | bytes 983040 | tf_op jit(solution)/shard_map/all_to_all | solution.py:76
  57.8 13.2 %all-to-all-done = f32[16,15,4,96]{3,2,1,0:T(4,128)S(1)} async-done(((f32[16,15,4,96]{3,2,1,0:T(4,128)}), f32[16,15,4,96]{3,2,1,0:T(4,128)S(1)}, u32[]{:S(2)}, u32[]{:S(2)}) %all-to-all-start) | async-done | bytes 368672 | tf_op jit(solution)/shard_map/all_to_all | solution.py:76
  71.0 7.4 %copy.79 = f32[15,4,16,96]{1,0,3,2:T(8,128)} copy(f32[15,4,16,96]{3,1,0,2:T(4,128)S(1)} %bitcast.159) | data formatting | bytes 737280
  78.4 9.6 %reshape.225 = f32[1536,60]{1,0:T(8,128)} reshape(f32[1536,15,4]{2,1,0:T(8,128)} %bitcast.157) | data formatting | bytes 737280
  89.0 16.0 %reduce-scatter.7.cloned.1.call-done = f32[768,60]{1,0:T(8,128)} async-done(((f32[1536,60]{1,0:T(8,128)}), f32[768,60]{1,0:T(8,128)}) %reduce-scatter.7.cloned.1.call-update) | async-done | bytes 184336
  105.0 5.3 %reshape.226 = bf16[768,15,4]{2,1,0:T(8,128)(2,1)} reshape(f32[768,60]{1,0:T(8,128)} %reduce-scatter.7.cloned.1.call-done) | data formatting | bytes 276480
  110.2 4.4 %copy.78 = bf16[15,4,768]{2,1,0:T(4,128)(2,1)S(1)} copy(bf16[15,4,768]{1,0,2:T(8,128)(2,1)} %bitcast.158) | data formatting | bytes 184320
  115.4 8.9 %fusion.1 = f32[15,6,1,128]{3,2,1,0:T(1,128)S(1)} fusion(bf16[15,6,128,128]{3,2,1,0:T(8,128)(2,1)} %param.17, f32[15,6,128]{2,1,0:T(8,128)S(1)} %mul.167, f32[15,6,128]{2,1,0:T(8,128)S(1)} %get-tuple-element.8, f32[15,6,128]{2,1,0:T(8,128)S(1)} %get-tuple-element.9, f32[15,6,128,1]{2,1,0,3:T(8,128)S(1)} %multiply_bitcast_fusion), kind=kOutput, calls=%fused_computation.3 | convolution fusion | flops 23592960 | bytes 3179520 | tf_op jit(solution)/shard_map/shk,shkv->shv/dot_general | solution.py:31
  124.6 22.5 %all-gather.1 = bf16[16,15,768]{2,1,0:T(8,128)(2,1)S(1)} all-gather(bf16[1,15,768]{2,1,0:T(8,128)(2,1)S(1)} %reshape.217), channel_id=1, replica_groups=mesh['ep'=16,'tp'=2] {'ep'}, dimensions={0}, use_global_device_ids=true | all-gather | bytes 391680 | tf_op jit(solution)/shard_map/all_gather | solution.py:90
  148.3 3.6 %all-to-all-start.1 = ((bf16[16,15,96]{2,1,0:T(8,128)(2,1)}), bf16[16,15,96]{2,1,0:T(8,128)(2,1)S(1)}, u32[]{:S(2)}, u32[]{:S(2)}) async-start(bf16[16,15,96]{2,1,0:T(8,128)(2,1)} %all_to_all.24), calls=%async_computation.1 | async-start | bytes 131072 | tf_op jit(solution)/shard_map/all_to_all | solution.py:94
  152.1 6.7 %all-to-all-done.1 = bf16[16,15,96]{2,1,0:T(8,128)(2,1)S(1)} async-done(((bf16[16,15,96]{2,1,0:T(8,128)(2,1)}), bf16[16,15,96]{2,1,0:T(8,128)(2,1)S(1)}, u32[]{:S(2)}, u32[]{:S(2)}) %all-to-all-start.1) | async-done | bytes 46112 | tf_op jit(solution)/shard_map/all_to_all | solution.py:94
  159.0 7.7 %psum.7 = bf16[15,1536]{1,0:T(8,128)(2,1)S(1)} all-reduce(bf16[15,1536]{1,0:T(8,128)(2,1)S(1)} %all_to_all.27), channel_id=1, replica_groups=mesh['ep'=16,'tp'=2] {'tp'}, use_global_device_ids=true, to_apply=%region_3.4 | all-reduce | flops 23040 | bytes 92160 | tf_op jit(solution)/shard_map/psum | solution.py:97
  167.9 14.8 %all_to_all.34 = bf16[16,6,1536]{2,1,0:T(8,128)(2,1)S(1)} all-to-all(bf16[16,6,1536]{2,1,0:T(8,128)(2,1)S(1)} %reshape.200), channel_id=1, replica_groups=mesh['ep'=16,'tp'=2] {'ep'}, dimensions={0} | all-to-all | bytes 589824 | tf_op jit(solution)/shard_map/all_to_all | solution.py:121
  183.0 1.4 fusion.5
  184.6 10.9 %reduce-scatter.5.cloned.1.call-done = bf16[16,1,6,768]{3,0,2,1:T(8,128)(2,1)} async-done(((bf16[16,1,6,1536]{3,0,2,1:T(8,128)(2,1)}), bf16[16,1,6,768]{3,0,2,1:T(8,128)(2,1)}) %reduce-scatter.5.cloned.1.call-update) | async-done | bytes 147472 | tf_op jit(solution)/shard_map/reduce_scatter | solution.py:132
  195.5 1.6 copy.74
  197.1 5.6 %all-to-all-start.3 = ((bf16[16,6,768]{2,1,0:T(8,128)(2,1)}), bf16[16,6,768]{2,1,0:T(8,128)(2,1)S(1)}, u32[]{:S(2)}, u32[]{:S(2)}) async-start(bf16[16,6,768]{2,1,0:T(8,128)(2,1)} %copy.74), calls=%async_computation.4 | async-start | bytes 393216 | tf_op jit(solution)/shard_map/all_to_all | solution.py:136
  202.8 6.7 %fusion = bf16[15,6,128,128]{3,2,1,0:T(8,128)(2,1)} fusion(bf16[15,6,128,128]{3,2,1,0:T(8,128)(2,1)} %param.17, f32[15,6,128]{2,1,0:T(8,128)S(1)} %mul.167, f32[15,6,128]{2,1,0:T(8,128)S(1)} %get-tuple-element.8, f32[15,6,128]{2,1,0:T(8,128)S(1)} %get-tuple-element.9), kind=kLoop, calls=%fused_computation.2 | loop fusion | flops 7372800 | bytes 6036480 | tf_op jit(solution)/shard_map/convert_element_type | solution.py:35
  209.5 2.3 %all-to-all-done.3 = bf16[16,6,768]{2,1,0:T(8,128)(2,1)S(1)} async-done(((bf16[16,6,768]{2,1,0:T(8,128)(2,1)}), bf16[16,6,768]{2,1,0:T(8,128)(2,1)S(1)}, u32[]{:S(2)}, u32[]{:S(2)}) %all-to-all-start.3) | async-done | bytes 147488 | tf_op jit(solution)/shard_map/all_to_all | solution.py:136
  (104 shorter events, 22.9 us)
Async XLA Ops:
  7.2 175.8 %copy-start = (bf16[1,256,1536]{2,1,0:T(8,128)(2,1)S(1)}, bf16[1,256,1536]{2,1,0:T(8,128)(2,1)}, u32[]{:S(2)}) copy-start(bf16[1,256,1536]{2,1,0:T(8,128)(2,1)} %param.31) | copy-start | bytes 2359300
  7.2 30.5 %copy-start.4 = (bf16[768,96]{0,1:T(8,128)(2,1)S(1)}, bf16[768,96]{0,1:T(8,128)(2,1)}, u32[]{:S(2)}) copy-start(bf16[768,96]{0,1:T(8,128)(2,1)} %param.19) | copy-start | bytes 442372
  47.4 9.9 %copy-start.10 = (s32[15,6]{0,1:T(8,128)S(1)}, s32[15,6]{0,1:T(8,128)}, u32[]{:S(2)}) copy-start(s32[15,6]{0,1:T(8,128)} %param.27) | copy-start | bytes 1084
  53.7 17.3 %all-to-all-start = ((f32[16,15,4,96]{3,2,1,0:T(4,128)}), f32[16,15,4,96]{3,2,1,0:T(4,128)S(1)}, u32[]{:S(2)}, u32[]{:S(2)}) async-start(f32[16,15,4,96]{3,2,1,0:T(4,128)} %copy.64), calls=%async_computation | async-start | bytes 983040 | tf_op jit(solution)/shard_map/all_to_all | solution.py:76
  57.3 47.7 %reduce-scatter.7.cloned.1.call-start = ((), (), s32[]{:S(2)}) async-start(), calls=%async_computation.7 | async-start | bytes 1179648
  57.4 30.9 %copy-start.6 = (s32[15,6]{1,0:T(8,128)}, s32[15,6]{1,0:T(8,128)S(1)}, u32[]{:S(2)}) copy-start(s32[15,6]{1,0:T(8,128)S(1)} %copy.69) | copy-start | bytes 1084
  78.4 10.6 %copy-start.8 = (f32[768]{0:T(1024)S(1)}, f32[768]{0:T(1024)}, u32[]{:S(2)}) copy-start(f32[768]{0:T(1024)} %param.23) | copy-start | bytes 9220
  88.2 26.4 %copy-start.13 = (s32[90]{0:T(128)}, s32[90]{0:T(128)S(1)}, u32[]{:S(2)}) copy-start(s32[90]{0:T(128)S(1)} %select_reduce_fusion) | copy-start | bytes 1084
  115.3 9.1 %copy-start.12 = (f32[128]{0:T(128)S(1)}, f32[128]{0:T(128)}, u32[]{:S(2)}) copy-start(f32[128]{0:T(128)} %param.24) | copy-start | bytes 1540
  115.3 31.9 %copy-start.5 = (bf16[768,96]{0,1:T(8,128)(2,1)S(1)}, bf16[768,96]{0,1:T(8,128)(2,1)}, u32[]{:S(2)}) copy-start(bf16[768,96]{0,1:T(8,128)(2,1)} %param.25) | copy-start | bytes 442372
  115.4 51.3 %copy-start.3 = (bf16[15,1536]{1,0:T(8,128)(2,1)S(1)}, bf16[15,1536]{1,0:T(8,128)(2,1)}, u32[]{:S(2)}) copy-start(bf16[15,1536]{1,0:T(8,128)(2,1)} %param.16) | copy-start | bytes 138244
  124.3 58.4 %copy-start.1 = (bf16[1,1536,256]{2,1,0:T(8,128)(2,1)S(1)}, bf16[1,1536,256]{2,1,0:T(8,128)(2,1)}, u32[]{:S(2)}) copy-start(bf16[1,1536,256]{2,1,0:T(8,128)(2,1)} %param.29) | copy-start | bytes 2359300
  124.3 58.7 %copy-start.2 = (bf16[1,1536,256]{2,1,0:T(8,128)(2,1)S(1)}, bf16[1,1536,256]{2,1,0:T(8,128)(2,1)}, u32[]{:S(2)}) copy-start(bf16[1,1536,256]{2,1,0:T(8,128)(2,1)} %param.30) | copy-start | bytes 2359300
  148.3 36.1 %copy-start.7 = (s32[15,6]{1,0:T(8,128)S(1)}, s32[15,6]{1,0:T(8,128)}, u32[]{:S(2)}) copy-start(s32[15,6]{1,0:T(8,128)} %copy-done.6) | copy-start | bytes 1084
  148.3 36.2 %copy-start.11 = (f32[15,6]{0,1:T(8,128)S(1)}, f32[15,6]{0,1:T(8,128)}, u32[]{:S(2)}) copy-start(f32[15,6]{0,1:T(8,128)} %param.28) | copy-start | bytes 1084
  148.3 36.3 %copy-start.14 = (s32[90]{0:T(128)S(1)}, s32[90]{0:T(128)}, u32[]{:S(2)}) copy-start(s32[90]{0:T(128)} %copy-done.13) | copy-start | bytes 1084
  148.3 10.5 %all-to-all-start.1 = ((bf16[16,15,96]{2,1,0:T(8,128)(2,1)}), bf16[16,15,96]{2,1,0:T(8,128)(2,1)S(1)}, u32[]{:S(2)}, u32[]{:S(2)}) async-start(bf16[16,15,96]{2,1,0:T(8,128)(2,1)} %all_to_all.24), calls=%async_computation.1 | async-start | bytes 131072 | tf_op jit(solution)/shard_map/all_to_all | solution.py:94
  151.9 43.6 %reduce-scatter.5.cloned.1.call-start = ((), (), s32[]{:S(2)}) async-start(), calls=%async_computation.6 | async-start | bytes 442368 | tf_op jit(solution)/shard_map/reduce_scatter | solution.py:132
  197.1 14.6 %all-to-all-start.3 = ((bf16[16,6,768]{2,1,0:T(8,128)(2,1)}), bf16[16,6,768]{2,1,0:T(8,128)(2,1)S(1)}, u32[]{:S(2)}, u32[]{:S(2)}) async-start(bf16[16,6,768]{2,1,0:T(8,128)(2,1)} %copy.74), calls=%async_computation.4 | async-start | bytes 393216 | tf_op jit(solution)/shard_map/all_to_all | solution.py:136
  202.8 9.9 %copy-start.9 = (pred[15,6]{1,0:T(8,128)(4,1)S(1)}, pred[15,6]{1,0:T(8,128)(4,1)}, u32[]{:S(2)}) copy-start(pred[15,6]{1,0:T(8,128)(4,1)} %get-tuple-element.6) | copy-start | bytes 274
Sparse Core Ops, SparseCore 0:
  88.1 16.7 reduce-scatter.6
  184.5 10.9 reduce-scatter.4
